TPU v7x, 32 devices: a whole 2x2x4 slice. The times are simulated.
32 devices in a mesh: sp: 8 (over z, y), tp: 4 (over x, core).
Axes of the slice: x: 2, y: 2, z: 4, core: 2. Of those that a mesh axis runs over, the one named last changes fastest.
Arguments:
- tokens: bfloat16 [3072, 2048], P('sp'), may hold values from -6 to 6
- norm_gain: float32 [2048], replicated, may hold values from 0.1 to 12
- w_query: bfloat16 [3, 512, 2048], P(None, 'tp'), may hold values from -0.125 to 0.125
- w_key: bfloat16 [3, 512, 2048], P(None, 'tp'), may hold values from -0.125 to 0.125
- w_value: bfloat16 [3, 512, 2048], P(None, 'tp'), may hold values from -0.125 to 0.125
- w_out: bfloat16 [512, 2048], P(None, 'tp'), may hold values from -0.25 to 0.25
Outputs:
- projected: bfloat16 [3072, 2048], P('sp', 'tp')
- log_weight: float32 [8, 3072], P('tp', 'sp')
All inputs are finite; a program needn't handle non-finite values.
Results may differ from a plain program's by a relative error of at most 0.006.
The roundings to bfloat16 on the way count: a program that leaves them out, or rounds other values in their place, can miss the bound.
Values may be sent and summed in bfloat16 or wider, within the bound.
A program may use at most 64 MiB of HBM per device.

v0:
```python
import functools
import math

import jax
import jax.numpy as jnp
from jax import lax
from jax.experimental import pallas as pl
from jax.experimental.pallas import tpu as pltpu
from jax.sharding import PartitionSpec as P

HEAD_DIM = 64
STEPS = 128
DILATIONS = (1, 4, 16)
NEG_BIG = -1e30
CHUNKS = 2
MESH = pl.DeviceIdType.MESH


def streams_of(dilation, rows):
    count = dilation
    while (rows // count) % 16:
        count //= 2
    return count


def kernel(
    n_sp, n_tp, total_slots, swap,
    tok_hbm, gain_hbm, wq_hbm, wk_hbm, wv_hbm,
    every_ref, logw_ref,
    tok, gain, w_all, normed, acc, qs1, qs2, qs3, ctx1, ctx2, ctx3,
    outs, lses, mix, going, stream, answer, back,
    in_sem, zs, zr, ys, yr, ms, mr, gs, gr, bs, br,
):
    rows, width = tok.shape
    cols = wq_hbm.shape[1]
    heads = cols // HEAD_DIM
    wide = acc.shape[2]
    me = lax.axis_index("sp")
    tp = lax.axis_index("tp")
    even = lax.rem(me, 2) == 0
    odd = lax.rem(me, 2) == 1
    partner = me + 1 - 2 * lax.rem(me, 2)
    ctxs = (ctx1, ctx2, ctx3)
    queries = (qs1, qs2, qs3)

    loads = {}
    def load(name, src, dst):
        loads[name] = pltpu.make_async_copy(src, dst, in_sem.at[len(loads)])
        loads[name].start()
    load("tok", tok_hbm, tok)
    load("gain", gain_hbm, gain)
    load(("q", 2), wq_hbm.at[2], w_all.at[2, 0:cols])
    for g in (2, 0, 1):
        load(("k", g), wk_hbm.at[g], w_all.at[g, cols:2 * cols])
        load(("v", g), wv_hbm.at[g], w_all.at[g, 2 * cols:3 * cols])
    for g in (1, 0):
        load(("q", g), wq_hbm.at[g], w_all.at[g, 0:cols])

    geo = []
    for g, dilation in enumerate(DILATIONS):
        s = ctxs[g].shape[0]
        m = rows // s
        halo = STEPS * dilation // s
        full = ctxs[g].shape[1] - m
        geo.append((s, m, halo, full))

    for g in range(2 if swap else 3):
        s, m, halo, full = geo[g]
        for p in range(s):
            ctxs[g][p, 0:full, :] = jnp.zeros((full, 2 * cols), jnp.bfloat16)

    barrier = pltpu.get_barrier_semaphore()
    if swap:
        for k in range(1, n_sp):
            pl.semaphore_signal(
                barrier, inc=1, device_id={"sp": lax.rem(me + k, n_sp)}, device_id_type=MESH)
    for by in () if swap else (1, 2):
        @pl.when(me >= by)
        def _():
            pl.semaphore_signal(barrier, inc=1, device_id={"sp": me - by}, device_id_type=MESH)
        @pl.when(me + by < n_sp)
        def _():
            pl.semaphore_signal(barrier, inc=1, device_id={"sp": me + by}, device_id_type=MESH)
    for k in range(1, n_tp):
        pl.semaphore_signal(barrier, inc=1, device_id={"tp": lax.rem(tp + k, n_tp)}, device_id_type=MESH)

    loads["tok"].wait()
    loads["gain"].wait()
    part = 32
    @pl.loop(0, rows // part)
    def _(j):
        at = pl.ds(pl.multiple_of(j * part, part), part)
        x = tok[at, :].astype(jnp.float32)
        scale = lax.rsqrt(jnp.mean(x * x, axis=-1, keepdims=True) + 1e-06)
        normed[at, :] = (x * scale * gain[...]).astype(jnp.bfloat16)

    NT = (((1,), (1,)), ((), ()))

    def key_value(g):
        s, m, halo, full = geo[g]
        loads["k", g].wait()
        loads["v", g].wait()
        both = lax.dot_general(
            normed[...], w_all[g, cols:3 * cols, :], NT, preferred_element_type=jnp.float32
        )
        if s == 1:
            ctxs[g][0, full:full + m, :] = both.astype(jnp.bfloat16)
            return
        acc[0, :, 0:cols] = both[:, 0:cols]
        acc[1, :, 0:cols] = both[:, cols:2 * cols]
        for p in range(s):
            for c in range(2):
                piece = acc[c, pl.ds(p, m, stride=s), :]
                ctxs[g][p, full:full + m, c * cols:(c + 1) * cols] = piece[:, 0:cols].astype(jnp.bfloat16)

    def query(g):
        s, m, halo, full = geo[g]
        loads["q", g].wait()
        got = lax.dot_general(
            normed[...], w_all[g, 0:cols, :], NT, preferred_element_type=jnp.float32
        )
        scale = 1.0 / math.sqrt(HEAD_DIM)
        if s == 1:
            queries[g][0] = got.astype(jnp.bfloat16) * jnp.bfloat16(scale)
            return
        acc[0, :, 0:cols] = got
        for p in range(s):
            piece = acc[0, pl.ds(p, m, stride=s), :]
            queries[g][p] = piece[:, 0:cols].astype(jnp.bfloat16) * jnp.bfloat16(scale)

    def region(g, back, streams, last=None):
        s, m, halo, full = geo[g]
        unit = m if g else STEPS
        stop = full - (back - 1) * unit if back else full + m
        size = unit if last is None else last
        return ctxs[g].at[streams, stop - size:stop, :]

    def z_copy(g, src, dst, slot, streams, last=None):
        return pltpu.make_async_remote_copy(
            region(g, src, streams, last), region(g, dst, streams, last),
            zs.at[slot], zr.at[slot], device_id={"sp": me + 2}, device_id_type=MESH)

    def y_copy(g, src, dst, slot, streams):
        return pltpu.make_async_remote_copy(
            region(g, src, streams), region(g, dst, streams),
            ys.at[slot], yr.at[slot], device_id={"sp": partner}, device_id_type=MESH)

    def on(cond, f):
        @pl.when(cond)
        def _():
            f()

    s3 = geo[2][0]
    per = s3 // CHUNKS
    full2 = pl.ds(0, geo[1][0])
    full1 = pl.ds(0, 1)
    tail3 = geo[2][2] - 5 * geo[2][1]
    tail2 = geo[1][2] - geo[1][1]
    z_list = []
    y_list = []
    for k in range(3):
        for c in range(CHUNKS):
            streams = pl.ds(c * per, per)
            z_list.append((2, 2 * k, k * CHUNKS + c, streams, tail3 if k == 2 else None))
            y_list.append((2, 2 * k, k * CHUNKS + c, streams))
    z_list += [(1, 0, 3 * CHUNKS, full2, tail2), (0, 0, 3 * CHUNKS + 1, full1, 0)]
    y_list += [(1, 0, 3 * CHUNKS, full2), (0, 0, 3 * CHUNKS + 1, full1)]

    def z_each(entry, has, act):
        g, src, slot, streams, tail = entry
        if tail is None:
            on(has, lambda: act(z_copy(g, src, src + 2, slot, streams)))
        else:
            if tail:
                on(has & even, lambda: act(z_copy(g, src, src + 2, slot, streams, tail)))
            on(has & odd, lambda: act(z_copy(g, src, src + 2, slot, streams)))

    def z_start(entry):
        z_each(entry, (me >= entry[1]) & (me + 2 < n_sp), lambda c: c.start())

    def z_sent(entry):
        z_each(entry, (me >= entry[1]) & (me + 2 < n_sp), lambda c: c.wait_send())

    def z_recv(entry):
        z_each(entry, me >= entry[1] + 2, lambda c: c.wait_recv())

    def y_even(entry, act):
        g, src, slot, streams = entry
        on(even & (me >= src), lambda: act(y_copy(g, src, src + 1, slot, streams)))

    def y_odd(entry, act):
        g, src, slot, streams = entry
        on(odd & (me >= src + 2), lambda: act(y_copy(g, src + 2, src + 1, slot, streams)))

    def y_recv(entry):
        g, src, slot, streams = entry
        on(me >= src + 1, lambda: y_copy(g, src, src + 1, slot, streams).wait_recv())

    start = lambda c: c.start()
    sent = lambda c: c.wait_send()
    z3 = lambda k: z_list[k * CHUNKS:(k + 1) * CHUNKS]
    y3 = lambda k: y_list[k * CHUNKS:(k + 1) * CHUNKS]

    def whole_stream():
        s, m, halo, full = geo[2]
        for name in "qkv":
            loads[name, 2].wait()
        got = lax.dot_general(normed[...], w_all[2], NT, preferred_element_type=jnp.float32)
        for c in range(3):
            acc[c] = got[:, c * cols:(c + 1) * cols]
        for p in range(s):
            for c in range(3):
                piece = acc[c, pl.ds(p, m, stride=s), :].astype(jnp.bfloat16)
                if c == 0:
                    piece = piece * jnp.bfloat16(1.0 / math.sqrt(HEAD_DIM))
                going[p, :, c * cols:(c + 1) * cols] = piece

    per_dev = geo[2][1]

    def mine_at(e):
        return pl.ds(pl.multiple_of(e * per_dev, 16), per_dev)

    def go(e, source):
        return pltpu.make_async_remote_copy(
            going.at[e], stream.at[mine_at(source), :], gs.at[e], gr.at[source],
            device_id={"sp": e}, device_id_type=MESH)

    def reply(e, source):
        return pltpu.make_async_remote_copy(
            answer.at[e * per_dev:(e + 1) * per_dev, :], back.at[source], bs.at[e], br.at[source],
            device_id={"sp": e}, device_id_type=MESH)

    def go_arrival(source):
        pltpu.make_async_remote_copy(
            going.at[source], stream.at[mine_at(source), :], gs.at[source], gr.at[source],
            device_id={"sp": source}, device_id_type=MESH).wait_recv()

    def reply_arrival(source):
        pltpu.make_async_remote_copy(
            answer.at[source * per_dev:(source + 1) * per_dev, :], back.at[source],
            bs.at[source], br.at[source],
            device_id={"sp": source}, device_id_type=MESH).wait_recv()

    def each_peer(f, peers=None):
        for e in peers or range(n_sp):
            on(me != e, lambda: f(e))

    if swap:
        whole_stream()
    else:
        key_value(2)
    if swap:
        peers = n_sp - 1 + n_tp - 1
    else:
        peers = jnp.minimum(me, 2) + jnp.minimum(n_sp - 1 - me, 2) + (n_tp - 1)
    pl.semaphore_wait(barrier, peers)
    if swap:
        each_peer(lambda e: go(e, me).start())
        stream[mine_at(me), :] = going[me]
    else:
        for c in range(CHUNKS):
            z_start(z3(0)[c])
            y_even(y3(0)[c], start)
    def near(entry):
        g, by, slot, last = entry
        streams = full2 if g else full1
        return pltpu.make_async_remote_copy(
            region(g, 0, streams, last), region(g, by, streams, last),
            zs.at[slot], zr.at[slot], device_id={"sp": me + by}, device_id_type=MESH)

    def near_start(entry):
        on(me + entry[1] < n_sp, lambda: near(entry).start())

    def near_sent(entry):
        on(me + entry[1] < n_sp, lambda: near(entry).wait_send())

    def near_recv(entry):
        on(me >= entry[1], lambda: near(entry).wait_recv())

    near_list = [(0, 1, 0, None), (1, 1, 1, None), (1, 2, 2, tail2)]
    if swap:
        key_value(0)
        near_start(near_list[0])
        key_value(1)
        near_start(near_list[1])
        near_start(near_list[2])
    else:
        key_value(1)
        z_start(z_list[-2])
        y_even(y_list[-2], start)
        key_value(0)
        z_start(z_list[-1])
        y_even(y_list[-1], start)
    for g in (0, 1) if swap else (0, 1, 2):
        query(g)

    def relay(k):
        for c in range(CHUNKS):
            z_recv(z3(k - 1)[c])
            z_start(z3(k)[c])
            y_odd(y3(k - 1)[c], start)
            y_even(y3(k)[c], start)

    lane_head = lax.broadcasted_iota(jnp.int32, (1, cols), 1) // HEAD_DIM

    def bias_of(g, height, length, first_key, offset):
        s = geo[g][0]
        halo = geo[g][2]
        ratio = DILATIONS[g] // s
        row = lax.broadcasted_iota(jnp.int32, (height, length), 0)
        col = lax.broadcasted_iota(jnp.int32, (height, length), 1)
        apart = row + offset - col
        step = apart // ratio
        valid = (apart >= 0) & (apart <= STEPS * ratio)
        if ratio > 1:
            valid = valid & (apart % ratio == 0)
        valid = valid & ((col + first_key) * s >= halo * s - me * rows)
        parts = []
        for h in range(heads):
            slot = (g * total_slots + tp * heads + h + 1).astype(jnp.float32)
            slope = jnp.exp2(jnp.full((1, 1), -8.0 / (3 * total_slots), jnp.float32) * slot)
            parts.append(jnp.where(valid, -slope * step.astype(jnp.float32), NEG_BIG))
        return jnp.concatenate(parts, axis=0) if heads > 1 else parts[0]

    def attend(q, keys, values, bias):
        height = q.shape[0]
        stacked = [jnp.where(lane_head == h, q, jnp.zeros_like(q)) for h in range(heads)]
        stacked = jnp.concatenate(stacked, axis=0) if heads > 1 else stacked[0]
        logits = lax.dot_general(stacked, keys, NT, preferred_element_type=jnp.float32) + bias
        top = jnp.max(logits, axis=-1, keepdims=True)
        e = jnp.exp(logits - top)
        total = jnp.sum(e, axis=-1, keepdims=True)
        lse = top + jnp.log(total)
        weights = (e * (1.0 / total)).astype(jnp.bfloat16)
        o = jnp.dot(weights, values, preferred_element_type=jnp.float32)
        out = o[0:height]
        log = jnp.broadcast_to(lse[0:height], (height, cols))
        for h in range(1, heads):
            mine = lane_head == h
            out = jnp.where(mine, o[h * height:(h + 1) * height], out)
            log = jnp.where(mine, lse[h * height:(h + 1) * height], log)
        return out, log

    def put(g, at, out, log):
        if cols < wide:
            out = jnp.concatenate([out] * (wide // cols), axis=1)
            log = jnp.concatenate([log] * (wide // cols), axis=1)
        outs[g, at, :] = out
        lses[g, at, :] = log

    def attend_group(g, first, count):
        s, m, halo, full = geo[g]
        base = full - halo
        bias = bias_of(g, m, halo + m, 0, halo)
        for p in range(first, first + count):
            out, log = attend(
                queries[g][p], ctxs[g][p, base:full + m, 0:cols],
                ctxs[g][p, base:full + m, cols:2 * cols], bias)
            put(g, pl.ds(p, m, stride=s), out, log)

    tile = STEPS

    def near_tile(j):
        base = geo[0][3] - STEPS + j * tile
        bias = bias_of(0, tile, tile + STEPS, j * tile, STEPS)
        out, log = attend(
            qs1[0, j * tile:(j + 1) * tile, :], ctx1[0, base:base + tile + STEPS, 0:cols],
            ctx1[0, base:base + tile + STEPS, cols:2 * cols], bias)
        put(0, pl.ds(j * tile, tile), out, log)

    def pass_on(entry, y_entry):
        z_recv(entry)
        y_odd(y_entry, start)

    same_head = (
        lax.broadcasted_iota(jnp.int32, (cols, cols), 0) // HEAD_DIM
        == lax.broadcasted_iota(jnp.int32, (cols, cols), 1) // HEAD_DIM
    ).astype(jnp.bfloat16)

    def stream_tile(j):
        stop = (j + 1) * tile
        s = geo[2][0]
        ratio = DILATIONS[2] // s
        row = lax.broadcasted_iota(jnp.int32, (tile, stop), 0)
        col = lax.broadcasted_iota(jnp.int32, (tile, stop), 1)
        apart = row + j * tile - col
        valid = (apart >= 0) & (apart <= STEPS * ratio) & (apart % ratio == 0)
        parts = []
        for h in range(heads):
            slot = (2 * total_slots + tp * heads + h + 1).astype(jnp.float32)
            slope = jnp.exp2(jnp.full((1, 1), -8.0 / (3 * total_slots), jnp.float32) * slot)
            parts.append(jnp.where(valid, -slope * (apart // ratio).astype(jnp.float32), NEG_BIG))
        bias = jnp.concatenate(parts, axis=0) if heads > 1 else parts[0]
        out, log = attend(
            stream[j * tile:stop, 0:cols], stream[0:stop, cols:2 * cols],
            stream[0:stop, 2 * cols:3 * cols], bias)
        high = log.astype(jnp.bfloat16).astype(jnp.float32)
        mid = (log - high).astype(jnp.bfloat16).astype(jnp.float32)
        low = log - high - mid
        place = lax.rem(lax.broadcasted_iota(jnp.int32, (1, cols), 1), HEAD_DIM)
        terms = jnp.where(place == 0, high, jnp.where(place == 1, mid, jnp.where(place == 2, low, 0.0)))
        answer[j * tile:stop, 0:cols] = out.astype(jnp.bfloat16)
        answer[j * tile:stop, cols:2 * cols] = terms.astype(jnp.bfloat16)

    if swap:
        for j in range(1, rows // tile):
            near_tile(j)
        each_peer(lambda e: go_arrival(e))
        done = 0
        for j in range(rows // tile):
            stream_tile(j)
            ready = (j + 1) * tile // per_dev
            each_peer(lambda e: reply(e, me).start(), range(done, ready))
            done = ready
        back[me] = answer[mine_at(me), :]
        near_recv(near_list[0])
        near_tile(0)
        near_recv(near_list[1])
        near_recv(near_list[2])
        attend_group(1, 0, geo[1][0])
        each_peer(lambda e: reply_arrival(e))
        for e in range(n_sp):
            log = jnp.dot(back[e, :, cols:2 * cols], same_head, preferred_element_type=jnp.float32)
            put(2, pl.ds(e, per_dev, stride=n_sp), back[e, :, 0:cols].astype(jnp.float32), log)
    else:
        relay(1)
        pass_on(z_list[-2], y_list[-2])
        pass_on(z_list[-1], y_list[-1])
        y_recv(y_list[-1])
        for j in range(rows // tile):
            near_tile(j)
        relay(2)
        y_recv(y_list[-2])
        attend_group(1, 0, geo[1][0])
        for c in range(CHUNKS):
            pass_on(z3(2)[c], y3(2)[c])
        for c in range(CHUNKS):
            for k in range(3):
                y_recv(y3(k)[c])
            attend_group(2, c * per, per)

    for j in range(rows // tile):
        at = pl.ds(j * tile, tile)
        logs = [lses[g, at, :] for g in range(3)]
        top = jnp.maximum(jnp.maximum(logs[0], logs[1]), logs[2])
        lw = top + jnp.log(sum(jnp.exp(l - top) for l in logs))
        mixed = sum(jnp.exp(logs[g] - lw) * outs[g, at, :] for g in range(3))
        mix[tp, at, :] = mixed[:, 0:cols].astype(jnp.bfloat16)
        flipped = lw.T
        for h in range(heads):
            logw_ref[h:h + 1, j * tile:(j + 1) * tile] = flipped[h * HEAD_DIM:h * HEAD_DIM + 1, :]

    def spread(k):
        to = lax.rem(tp + k, n_tp)
        return pltpu.make_async_remote_copy(
            mix.at[tp], mix.at[tp], ms.at[k - 1], mr.at[k - 1],
            device_id={"tp": to}, device_id_type=MESH)

    def arrival(k):
        source = lax.rem(tp + n_tp - k, n_tp)
        return pltpu.make_async_remote_copy(
            mix.at[source], mix.at[source], ms.at[k - 1], mr.at[k - 1],
            device_id={"tp": lax.rem(tp + k, n_tp)}, device_id_type=MESH)

    for k in range(1, n_tp):
        spread(k).start()
    for k in range(1, n_tp):
        arrival(k).wait_recv()
    for t in range(n_tp):
        every_ref[:, t * cols:(t + 1) * cols] = mix[t]

    for k in range(1, n_tp):
        spread(k).wait_send()
    if swap:
        each_peer(lambda e: go(e, me).wait_send())
        each_peer(lambda e: reply(e, me).wait_send())
        for entry in near_list:
            near_sent(entry)
    for entry in () if swap else z_list:
        z_sent(entry)
    for entry in () if swap else y_list:
        y_even(entry, sent)
        y_odd(entry, sent)


def project(every_ref, w_ref, log_ref, proj_ref, logw_ref):
    proj_ref[...] = jnp.dot(
        every_ref[...], w_ref[...], preferred_element_type=jnp.float32
    ).astype(jnp.bfloat16)
    logw_ref[...] = log_ref[...]


def solution(mesh):
    n_sp, n_tp = mesh.shape["sp"], mesh.shape["tp"]

    def per_device(tokens, norm_gain, w_query, w_key, w_value, w_out):
        rows, width = tokens.shape
        cols = w_query.shape[1]
        out_cols = w_out.shape[1]
        heads = cols // HEAD_DIM
        wide = max(cols, 128)
        bf, f32 = jnp.bfloat16, jnp.float32
        counts = [streams_of(d, rows) for d in DILATIONS]
        m = [rows // s for s in counts]
        slots = 3 * CHUNKS + 2
        swap = n_sp == counts[2] and cols % 128 == 0
        vmem = pltpu.VMEM
        dma = pltpu.SemaphoreType.DMA
        mixed, logs = pl.pallas_call(
            functools.partial(kernel, n_sp, n_tp, heads * n_tp, swap),
            out_shape=(
                jax.ShapeDtypeStruct((rows, n_tp * cols), bf),
                jax.ShapeDtypeStruct((heads, rows), f32),
            ),
            in_specs=[pl.BlockSpec(memory_space=pl.ANY)] * 5,
            out_specs=(pl.BlockSpec(memory_space=pltpu.VMEM),) * 2,
            scratch_shapes=[
                vmem((rows, width), bf),
                vmem((1, width), f32),
                vmem((3, 3 * cols, width), bf),
                vmem((rows, width), bf),
                vmem((3, rows, wide), f32),
                vmem((counts[0], m[0], cols), bf),
                vmem((counts[1], m[1], cols), bf),
                vmem((counts[2], m[2], cols), bf),
                vmem((1, 2 * STEPS + rows, 2 * cols), bf),
                vmem((counts[1], 3 * m[1], 2 * cols), bf),
                vmem((counts[2], 7 * m[2], 2 * cols), bf),
                vmem((3, rows, wide), f32),
                vmem((3, rows, wide), f32),
                vmem((n_tp, rows, cols), bf),
                vmem((counts[2], m[2], 3 * cols), bf),
                vmem((rows, 3 * cols), bf),
                vmem((rows, 2 * cols), bf),
                vmem((counts[2], m[2], 2 * cols), bf),
                dma((12,)),
                dma((slots,)), dma((slots,)), dma((slots,)), dma((slots,)),
                dma((n_tp - 1,)), dma((n_tp - 1,)),
                dma((n_sp,)), dma((n_sp,)), dma((n_sp,)), dma((n_sp,)),
            ],
            compiler_params=pltpu.CompilerParams(
                collective_id=0, has_side_effects=True, vmem_limit_bytes=60 * 1024 * 1024
            ),
        )(tokens, norm_gain.reshape(1, width), w_query, w_key, w_value)
        return pl.pallas_call(
            project,
            out_shape=(
                jax.ShapeDtypeStruct((rows, out_cols), bf),
                jax.ShapeDtypeStruct((heads, rows), f32),
            ),
        )(mixed, w_out, logs)

    in_specs = (
        P("sp", None),
        P(),
        P(None, "tp", None),
        P(None, "tp", None),
        P(None, "tp", None),
        P(None, "tp"),
    )
    out_specs = (P("sp", "tp"), P("tp", "sp"))
    return jax.shard_map(
        per_device, mesh=mesh, in_specs=in_specs, out_specs=out_specs, check_vma=False
    )
```

profile of v0, /device:TPU:25, one launch (start us, length us, event | category | flops | bytes accessed | tf_op | source)
XLA Modules:
  0.0 33.9 jit_solution(11444638977039335173)
XLA Ops:
  0.6 31.0 %shard_map.77 = (bf16[384,512]{1,0:T(8,128)(2,1)}, f32[2,384]{1,0:T(2,128)}) custom-call(bf16[384,2048]{1,0:T(8,128)(2,1)} %tok_hbm.1, f32[1,2048]{1,0:T(1,128)} %bitcast.1, bf16[3,128,2048]{2,1,0:T(8,128)(2,1)} %wq_hbm.1, bf16[3,128,2048]{2,1,0:T(8,128)(2,1)} %wk_hbm.1, bf16[3,128,2048]{2,1,0:T(8,128)(2,1)} %wv_hbm.1), custom_call_target="tpu_custom_call" | custom-call | tf_op jit(solution)/shard_map/pallas_call | solution.py:509
  31.7 2.3 %shard_map.78 = (bf16[384,512]{1,0:T(8,128)(2,1)}, f32[2,384]{1,0:T(2,128)}) custom-call(bf16[384,512]{1,0:T(8,128)(2,1)} %get-tuple-element.4.every_ref, bf16[512,512]{1,0:T(8,128)(2,1)} %w_ref.1, f32[2,384]{1,0:T(2,128)} %get-tuple-element.5.log_ref), custom_call_target="tpu_custom_call" | custom-call | tf_op jit(solution)/shard_map/pallas_call | solution.py:545
where the time goes:
time: 34.1 us; the launch traced here: 33.9 us
  Pallas kernels  33.3 us (98%)
  between operations  0.64 us (2%)
    pallas_call x1, Pallas kernels, per_device(): pl.pallas_call(functools.partial(kernel, n_sp, n_tp, heads * n_tp, swap),...  31 us
    pallas_call x1, Pallas kernels, per_device(): pl.pallas_call(project, out_shape=(jax.ShapeDtypeStruct((rows, out_cols),...  2.27 us

commit v1 on v0

--- a/solution.py
+++ b/solution.py
@@ -13,6 +13,8 @@
 DILATIONS = (1, 4, 16)
 NEG_BIG = -1e30
 CHUNKS = 2
+STORE_LIMIT = 8 * 1024 * 1024
+VMEM_LIMIT = 56098816
 MESH = pl.DeviceIdType.MESH
 
 
@@ -483,6 +485,494 @@
         y_odd(entry, sent)
 
 
+LANES = 128
+NT = (((1,), (1,)), ((), ()))
+
+
+def split_kernel(
+    n_sp, n_tp, total_slots,
+    tok_hbm, gain_hbm, wq_hbm, wk_hbm, wv_hbm, wo_hbm,
+    proj_ref, logw_ref,
+    tok, gain, w_all, w_out, normed, acc, q1, q2, ctx1, ctx2, going, stream, qfar,
+    answer, answer_far, lse_near, lse_far, back, back_far, back_lse, back_far_lse,
+    b0, b0_first, b1, b2, b3, out0, log0, part_o, part_l, mix, nat, lw_nat,
+    in_sem, gs, gr, fs, fr, ns, nr, as_, ar, ls, lr, bs, br, cs, cr, ms, mr,
+):
+    rows, width = tok.shape
+    cols = wq_hbm.shape[1]
+    heads = cols // HEAD_DIM
+    classes = going.shape[0]
+    per = rows // classes
+    ratio = DILATIONS[2] // classes
+    tile = STEPS
+    me = lax.axis_index("sp")
+    tp = lax.axis_index("tp")
+    mine = lax.rem(me, classes)
+    base = me - mine
+    upper = me >= classes
+    lower = me < classes
+
+    loads = {}
+
+    def load(name, src, dst):
+        loads[name] = pltpu.make_async_copy(src, dst, in_sem.at[len(loads)])
+        loads[name].start()
+
+    for c in range(classes):
+        at = pl.ds(c * per, per)
+        load(("tok", c), tok_hbm.at[at], tok.at[at])
+        if c == 0:
+            load("gain", gain_hbm, gain)
+    slot = 0
+    weights = (
+        (2, "q"), (2, "k"), (2, "v"), (1, "k"), (1, "v"), (0, "k"), (0, "v"), (1, "q"), (0, "q"))
+    for g, kind in weights:
+        src = {"q": wq_hbm, "k": wk_hbm, "v": wv_hbm}[kind]
+        load((kind, g), src.at[g], w_all.at[slot * cols:(slot + 1) * cols])
+        slot += 1
+    load("out", wo_hbm, w_out)
+
+    barrier = pltpu.get_barrier_semaphore()
+    for k in range(1, n_sp):
+        pl.semaphore_signal(
+            barrier, inc=1, device_id={"sp": lax.rem(me + k, n_sp)}, device_id_type=MESH)
+    for k in range(1, n_tp):
+        pl.semaphore_signal(
+            barrier, inc=1, device_id={"tp": lax.rem(tp + k, n_tp)}, device_id_type=MESH)
+
+    @pl.when(me == 0)
+    def _():
+        ctx1[0:tile, :] = jnp.zeros((tile, 2 * cols), jnp.bfloat16)
+        for p in range(classes):
+            ctx2[p, 0:tile, :] = jnp.zeros((tile, 2 * cols), jnp.bfloat16)
+
+    @pl.when(me == 1)
+    def _():
+        for p in range(classes):
+            ctx2[p, 0:tile - per, :] = jnp.zeros((tile - per, 2 * cols), jnp.bfloat16)
+
+    def bias(g, height, first, last, offset, step, key_limit):
+        row = lax.broadcasted_iota(jnp.int32, (height, last - first), 0)
+        col = lax.broadcasted_iota(jnp.int32, (height, last - first), 1) + first
+        apart = row + offset - col
+        valid = (apart >= 0) & (apart <= STEPS * step)
+        shift = step.bit_length() - 1
+        if step > 1:
+            valid = valid & ((apart & (step - 1)) == 0)
+        if key_limit is not None:
+            valid = valid & (col >= key_limit)
+        far = lax.shift_right_arithmetic(apart, shift).astype(jnp.float32)
+        parts = []
+        for h in range(heads):
+            slot = (g * total_slots + tp * heads + h + 1).astype(jnp.float32)
+            slope = jnp.exp2(jnp.full((1, 1), -8.0 / (3 * total_slots), jnp.float32) * slot)
+            parts.append(jnp.where(valid, -slope * far, NEG_BIG))
+        return parts
+
+    def keep(ref, parts):
+        height, length = parts[0].shape
+        for h in range(heads):
+            ref[h * height:(h + 1) * height, 0:length] = parts[h]
+
+    def near_keys(k):
+        return -(-(k + 1) * per // LANES) * LANES
+
+    def far_keys(k):
+        return max(0, (rows + k * per - STEPS * ratio) // LANES * LANES)
+
+    keep(b0, bias(0, tile, 0, 2 * tile, tile, 1, None))
+    keep(b0_first, bias(0, tile, 0, 2 * tile, tile, 1, jnp.where(me == 0, tile, 0)))
+    keep(b1, bias(1, per, 0, tile + per, tile, 1, jnp.maximum(tile - me * per, 0)))
+    for k in range(classes):
+        keep(b2.at[k], bias(2, per, 0, near_keys(k), k * per, ratio, None))
+        keep(b3.at[k], bias(2, per, far_keys(k), rows, rows + k * per, ratio, None))
+
+    loads["gain"].wait()
+    part = 32
+    for c in range(classes):
+        loads["tok", c].wait()
+        for j in range(per // part):
+            at = pl.ds(c * per + j * part, part)
+            x = tok[at, :].astype(jnp.float32)
+            scale = lax.rsqrt(jnp.mean(x * x, axis=-1, keepdims=True) + 1e-06)
+            normed[at, :] = (x * scale * gain[...]).astype(jnp.bfloat16)
+
+    def product(first, count):
+        for g, kind in weights[first:first + count]:
+            loads[kind, g].wait()
+        return lax.dot_general(
+            normed[...], w_all[first * cols:(first + count) * cols, :], NT,
+            preferred_element_type=jnp.float32)
+
+    def by_class(n, p):
+        return acc[n, pl.ds(p, per, stride=classes), :].astype(jnp.bfloat16)
+
+    scaling = jnp.bfloat16(1.0 / math.sqrt(HEAD_DIM))
+    got = product(0, 3)
+    for n in range(3):
+        acc[n] = got[:, n * cols:(n + 1) * cols]
+    for p in range(classes):
+        going[p, :, 0:cols] = by_class(0, p) * scaling
+        going[p, :, cols:2 * cols] = by_class(1, p)
+        going[p, :, 2 * cols:3 * cols] = by_class(2, p)
+
+    def slice_of(k):
+        return pl.ds(pl.multiple_of(k * per, 16), per)
+
+    def remote(src, dst, send, recv, sp):
+        return pltpu.make_async_remote_copy(
+            src, dst, send, recv, device_id={"sp": sp}, device_id_type=MESH)
+
+    def go(c, source):
+        return remote(going.at[c], stream.at[slice_of(source), :], gs.at[c], gr.at[source], base + c)
+
+    def go_far(c, source):
+        return remote(going.at[c, :, 0:cols], qfar.at[source], fs.at[c], fr.at[source], c)
+
+    def reply(e, source):
+        return remote(answer.at[e], back.at[source], as_.at[e], ar.at[source], base + e)
+
+    def reply_lse(e, source):
+        return remote(lse_near.at[e], back_lse.at[source], ls.at[e], lr.at[source], base + e)
+
+    def reply_far(e, source):
+        return remote(
+            answer_far.at[e], back_far.at[source], bs.at[e], br.at[source], classes + e)
+
+    def reply_far_lse(e, source):
+        return remote(
+            lse_far.at[e], back_far_lse.at[source], cs.at[e], cr.at[source], classes + e)
+
+    def when(cond, f):
+        @pl.when(cond)
+        def _():
+            f()
+
+    def each_peer(f):
+        for e in range(classes):
+            when(mine != e, lambda: f(e))
+
+    tail = tile - per
+    full2 = pl.ds(0, classes)
+
+    def near(n):
+        if n == 0:
+            src, dst, by = ctx1.at[rows:rows + tile, :], ctx1.at[0:tile, :], 1
+        elif n == 1:
+            src, dst, by = ctx2.at[full2, tile:tile + per, :], ctx2.at[full2, tail:tile, :], 1
+        else:
+            src, dst, by = ctx2.at[full2, tile + per - tail:tile + per, :], ctx2.at[full2, 0:tail, :], 2
+        return by, remote(src, dst, ns.at[n], nr.at[n], me + by)
+
+    def near_start(n):
+        by, copy = near(n)
+        when(me + by < n_sp, copy.start)
+
+    def near_sent(n):
+        by, copy = near(n)
+        when(me + by < n_sp, copy.wait_send)
+
+    def near_arrival(n):
+        by, copy = near(n)
+        when(me >= by, copy.wait_recv)
+
+    pl.semaphore_wait(barrier, n_sp - 1 + n_tp - 1)
+
+    @pl.when(upper)
+    def _():
+        for c in range(classes):
+            go_far(c, mine).start()
+
+    each_peer(lambda e: go(e, mine).start())
+    stream[slice_of(mine), :] = going[mine]
+
+    got = product(3, 4)
+    for n in range(2):
+        acc[n] = got[:, n * cols:(n + 1) * cols]
+    for p in range(classes):
+        for n in range(2):
+            ctx2[p, tile:tile + per, n * cols:(n + 1) * cols] = by_class(n, p)
+    ctx1[tile:tile + rows, :] = got[:, 2 * cols:4 * cols].astype(jnp.bfloat16)
+
+    got = product(7, 2)
+    acc[2] = got[:, 0:cols]
+    for p in range(classes):
+        q2[p] = by_class(2, p) * scaling
+    q1[...] = got[:, cols:2 * cols].astype(jnp.bfloat16) * scaling
+
+    lane = lax.broadcasted_iota(jnp.int32, (1, cols), 1)
+    lane_head = lane // HEAD_DIM
+    lane_turn = lax.rem(lane, heads)
+
+    def attend(q, keys, values, bias_ref, length):
+        height = q.shape[0]
+        stacked = jnp.concatenate(
+            [jnp.where(lane_head == h, q, jnp.zeros_like(q)) for h in range(heads)], axis=0)
+        logits = lax.dot_general(stacked, keys, NT, preferred_element_type=jnp.float32)
+        logits = logits + bias_ref[0:heads * height, 0:length]
+        top = jnp.max(logits, axis=-1, keepdims=True)
+        e = jnp.exp(logits - top)
+        total = jnp.sum(e, axis=-1, keepdims=True)
+        o = jnp.dot(e.astype(jnp.bfloat16), values, preferred_element_type=jnp.float32)
+        o = o * (1.0 / total)
+        lse = top + jnp.log(total)
+        out = o[0:height]
+        for h in range(1, heads):
+            out = jnp.where(lane_head == h, o[h * height:(h + 1) * height], out)
+        return out, [lse[h * height:(h + 1) * height] for h in range(heads)]
+
+    def lanes_of(lse, pattern):
+        log = jnp.broadcast_to(lse[0], (lse[0].shape[0], cols))
+        for h in range(1, heads):
+            log = jnp.where(pattern == h, lse[h], log)
+        return log
+
+    def pack(ref, k, lse):
+        ref[k, :, 0:per] = lanes_of(lse, lane_turn).T[0:heads, :]
+
+    def unpack(ref, k):
+        row = ref[k]
+        wide = [jnp.broadcast_to(row[h:h + 1, :], (HEAD_DIM, LANES)) for h in range(heads)]
+        return jnp.concatenate(wide, axis=0).T[0:per, :]
+
+    def near_tile(j, bias_ref):
+        first = j * tile
+        out, lse = attend(
+            q1[first:first + tile, :], ctx1[first:first + 2 * tile, 0:cols],
+            ctx1[first:first + 2 * tile, cols:2 * cols], bias_ref, 2 * tile)
+        out0[first:first + tile, :] = out
+        log0[first:first + tile, :] = lanes_of(lse, lane_head)
+
+    for j in range(1, rows // tile):
+        near_tile(j, b0)
+    near_start(1)
+    near_start(2)
+    near_start(0)
+
+    def go_arrival(k):
+        go(k, k).wait_recv()
+
+    each_peer(go_arrival)
+    for k in range(classes):
+        stop = near_keys(k)
+        out, lse = attend(
+            stream[k * per:(k + 1) * per, 0:cols], stream[0:stop, cols:2 * cols],
+            stream[0:stop, 2 * cols:3 * cols], b2.at[k], stop)
+        answer[k] = out.astype(jnp.bfloat16)
+        pack(lse_near, k, lse)
+    each_peer(lambda e: (reply(e, mine).start(), reply_lse(e, mine).start()))
+    back[mine] = answer[mine]
+    back_lse[mine] = lse_near[mine]
+
+    @pl.when(lower)
+    def _():
+        for k in range(classes):
+            go_far(k, k).wait_recv()
+        for k in range(classes):
+            first = far_keys(k)
+            out, lse = attend(
+                qfar[k], stream[first:rows, cols:2 * cols],
+                stream[first:rows, 2 * cols:3 * cols], b3.at[k], rows - first)
+            answer_far[k] = out.astype(jnp.bfloat16)
+            pack(lse_far, k, lse)
+        for k in range(classes):
+            reply_far(k, mine).start()
+            reply_far_lse(k, mine).start()
+
+    near_arrival(0)
+    near_tile(0, b0_first)
+    near_arrival(1)
+    near_arrival(2)
+    near_parts = []
+    for p in range(classes):
+        near_parts.append(attend(
+            q2[p], ctx2[p, :, 0:cols], ctx2[p, :, cols:2 * cols], b1, tile + per))
+    for p in range(classes):
+        out, lse = near_parts[p]
+        part_o[p] = out
+        part_l[p] = lanes_of(lse, lane_head)
+
+    def merge(logs, outs):
+        top = functools.reduce(jnp.maximum, logs)
+        log = top + jnp.log(sum(jnp.exp(l - top) for l in logs))
+        return log, sum(jnp.exp(l - log) * o for l, o in zip(logs, outs))
+
+    each_peer(lambda e: (reply(e, e).wait_recv(), reply_lse(e, e).wait_recv()))
+    for p in range(classes):
+        at = pl.ds(p, per, stride=classes)
+        log, out = merge(
+            [log0[at, :], part_l[p], unpack(back_lse, p)],
+            [out0[at, :], part_o[p], back[p].astype(jnp.float32)])
+        part_l[p] = log
+        part_o[p] = out
+
+    def spread(k, c):
+        return pltpu.make_async_remote_copy(
+            mix.at[tp, c], mix.at[tp, c], ms.at[k - 1, c], mr.at[k - 1, c],
+            device_id={"tp": lax.rem(tp + k, n_tp)}, device_id_type=MESH)
+
+    def spread_arrival(k, c):
+        source = lax.rem(tp + n_tp - k, n_tp)
+        return pltpu.make_async_remote_copy(
+            mix.at[source, c], mix.at[source, c], ms.at[k - 1, c], mr.at[k - 1, c],
+            device_id={"tp": lax.rem(tp + k, n_tp)}, device_id_type=MESH)
+
+    def finish(c):
+        @pl.when(upper)
+        def _():
+            reply_far(c, c).wait_recv()
+            reply_far_lse(c, c).wait_recv()
+            log, out = merge(
+                [part_l[c], unpack(back_far_lse, c)],
+                [part_o[c], back_far[c].astype(jnp.float32)])
+            part_l[c] = log
+            part_o[c] = out
+
+        mix[tp, c] = part_o[c].astype(jnp.bfloat16)
+        lw_nat[pl.ds(c, per, stride=classes), :] = part_l[c]
+        for k in range(1, n_tp):
+            spread(k, c).start()
+
+    def project_class(c):
+        for k in range(1, n_tp):
+            spread_arrival(k, c).wait_recv()
+        mixed = jnp.concatenate([mix[t, c] for t in range(n_tp)], axis=1)
+        got = jnp.dot(mixed, w_out[...], preferred_element_type=jnp.float32)
+        for n in range(nat.shape[0]):
+            nat[n, pl.ds(c, per, stride=classes), :] = got[:, n * LANES:(n + 1) * LANES]
+
+    finish(0)
+    finish(1)
+    loads["out"].wait()
+    for c in range(classes):
+        if c + 2 < classes:
+            finish(c + 2)
+        project_class(c)
+    for n in range(nat.shape[0]):
+        proj_ref[:, n * LANES:(n + 1) * LANES] = nat[n].astype(jnp.bfloat16)
+    for j in range(rows // tile):
+        flipped = lw_nat[j * tile:(j + 1) * tile, :].T
+        for h in range(heads):
+            logw_ref[h:h + 1, j * tile:(j + 1) * tile] = flipped[h * HEAD_DIM:h * HEAD_DIM + 1, :]
+
+    for c in range(classes):
+        for k in range(1, n_tp):
+            spread(k, c).wait_send()
+    each_peer(lambda e: (
+        go(e, mine).wait_send(), reply(e, mine).wait_send(), reply_lse(e, mine).wait_send()))
+
+    @pl.when(upper)
+    def _():
+        for c in range(classes):
+            go_far(c, mine).wait_send()
+
+    @pl.when(lower)
+    def _():
+        for c in range(classes):
+            reply_far(c, mine).wait_send()
+            reply_far_lse(c, mine).wait_send()
+
+    for n in range(3):
+        near_sent(n)
+
+
+def store(proj_ref, logw_ref, proj_out, logw_out, sem):
+    copies = [
+        pltpu.make_async_copy(proj_ref, proj_out, sem.at[0]),
+        pltpu.make_async_copy(logw_ref, logw_out, sem.at[1]),
+    ]
+    for copy in copies:
+        copy.start()
+    for copy in copies:
+        copy.wait()
+
+
+def split_call(n_sp, n_tp, tokens, norm_gain, w_query, w_key, w_value, w_out):
+    rows, width = tokens.shape
+    cols = w_query.shape[1]
+    out_cols = w_out.shape[1]
+    heads = cols // HEAD_DIM
+    classes = n_sp // 2
+    per = rows // classes
+    bf, f32 = jnp.bfloat16, jnp.float32
+    vmem = pltpu.VMEM
+    dma = pltpu.SemaphoreType.DMA
+    lanes2 = heads * per
+    shapes = (
+        jax.ShapeDtypeStruct((rows, out_cols), bf),
+        jax.ShapeDtypeStruct((heads, rows), f32),
+    )
+    results = pl.pallas_call(
+        functools.partial(split_kernel, n_sp, n_tp, heads * n_tp),
+        out_shape=shapes,
+        in_specs=[pl.BlockSpec(memory_space=pltpu.HBM)] * 6,
+        out_specs=(pl.BlockSpec(memory_space=pltpu.VMEM),) * 2,
+        scratch_shapes=[
+            vmem((rows, width), bf),
+            vmem((1, width), f32),
+            vmem((9 * cols, width), bf),
+            vmem(w_out.shape, bf),
+            vmem((rows, width), bf),
+            vmem((3, rows, cols), f32),
+            vmem((rows, cols), bf),
+            vmem((classes, per, cols), bf),
+            vmem((STEPS + rows, 2 * cols), bf),
+            vmem((classes, STEPS + per, 2 * cols), bf),
+            vmem((classes, per, 3 * cols), bf),
+            vmem((rows, 3 * cols), bf),
+            vmem((classes, per, cols), bf),
+            vmem((classes, per, cols), bf),
+            vmem((classes, per, cols), bf),
+            vmem((classes, heads, LANES), f32),
+            vmem((classes, heads, LANES), f32),
+            vmem((classes, per, cols), bf),
+            vmem((classes, per, cols), bf),
+            vmem((classes, heads, LANES), f32),
+            vmem((classes, heads, LANES), f32),
+            vmem((heads * STEPS, 2 * STEPS), f32),
+            vmem((heads * STEPS, 2 * STEPS), f32),
+            vmem((lanes2, STEPS + per), f32),
+            vmem((classes, lanes2, rows), f32),
+            vmem((classes, lanes2, rows), f32),
+            vmem((rows, cols), f32),
+            vmem((rows, cols), f32),
+            vmem((classes, per, cols), f32),
+            vmem((classes, per, cols), f32),
+            vmem((n_tp, classes, per, cols), bf),
+            vmem((out_cols // LANES, rows, LANES), f32),
+            vmem((rows, cols), f32),
+            dma((11 + classes,)),
+            dma((classes,)), dma((classes,)), dma((classes,)), dma((classes,)),
+            dma((3,)), dma((3,)),
+            dma((classes,)), dma((classes,)), dma((classes,)), dma((classes,)),
+            dma((classes,)), dma((classes,)), dma((classes,)), dma((classes,)),
+            dma((n_tp - 1, classes)), dma((n_tp - 1, classes)),
+        ],
+        compiler_params=pltpu.CompilerParams(
+            collective_id=0, has_side_effects=True, vmem_limit_bytes=VMEM_LIMIT
+        ),
+    )(tokens, norm_gain.reshape(1, width), w_query, w_key, w_value, w_out)
+    return pl.pallas_call(
+        store,
+        out_shape=shapes,
+        in_specs=[pl.BlockSpec(memory_space=pltpu.VMEM)] * 2,
+        out_specs=(pl.BlockSpec(memory_space=pl.ANY),) * 2,
+        scratch_shapes=[pltpu.SemaphoreType.DMA((2,))],
+        compiler_params=pltpu.CompilerParams(vmem_limit_bytes=STORE_LIMIT),
+    )(*results)
+
+
+def splits(n_sp, n_tp, rows, cols, out_cols):
+    classes = n_sp // 2
+    if n_sp % 2 or classes != DILATIONS[1] or DILATIONS[2] % classes:
+        return False
+    if cols != LANES or LANES % HEAD_DIM or rows % (classes * 32) or rows % STEPS or out_cols % LANES:
+        return False
+    per = rows // classes
+    window = STEPS * DILATIONS[2] // classes
+    return per <= STEPS <= 2 * per and classes * per <= window
+
+
 def project(every_ref, w_ref, log_ref, proj_ref, logw_ref):
     proj_ref[...] = jnp.dot(
         every_ref[...], w_ref[...], preferred_element_type=jnp.float32
@@ -499,6 +989,8 @@
         out_cols = w_out.shape[1]
         heads = cols // HEAD_DIM
         wide = max(cols, 128)
+        if splits(n_sp, n_tp, rows, cols, out_cols):
+            return split_call(n_sp, n_tp, tokens, norm_gain, w_query, w_key, w_value, w_out)
         bf, f32 = jnp.bfloat16, jnp.float32
         counts = [streams_of(d, rows) for d in DILATIONS]
         m = [rows // s for s in counts]

time: 34.1 us -> 29.3 us (0.86)
  the two profiles are of different devices: /device:TPU:25 before, /device:TPU:0 now
where the time goes in v1:
time: 29.3 us; the launch traced here: 29.1 us
  Pallas kernels  27.8 us (95%)
  local copies, waits for them, and re-layouts  0.69 us (2%)
  between operations  0.65 us (2%)
    pallas_call x1, Pallas kernels, split_call(): pl.pallas_call(functools.partial(split_kernel, n_sp, n_tp, heads * n_tp),...  27 us
    pallas_call x1, Pallas kernels, split_call(): pl.pallas_call(store, out_shape=shapes, in_specs=[pl.BlockSpec(memory_spa...  0.77 us
    unnamed x2, local copies, waits for them, and re-layouts  0.69 us

profile of v1, /device:TPU:0, one launch (start us, length us, event | category | flops | bytes accessed | tf_op | source)
XLA Modules:
  0.0 29.1 jit_solution(6197964387511678879)
XLA Ops:
  0.6 0.0 copy-start
  0.6 0.7 %copy-done = f32[2048]{0:T(1024)S(1)} copy-done((f32[2048]{0:T(1024)S(1)}, f32[2048]{0:T(1024)}, u32[]{:S(2)}) %copy-start) | copy-done | bytes 8216
  1.3 27.0 %shard_map.77 = (bf16[384,512]{1,0:T(8,128)(2,1)S(1)}, f32[2,384]{1,0:T(2,128)S(1)}) custom-call(bf16[384,2048]{1,0:T(8,128)(2,1)} %tok_hbm.1, f32[1,2048]{1,0:T(1,128)S(1)} %bitcast.1, bf16[3,128,2048]{2,1,0:T(8,128)(2,1)} %wq_hbm.1, bf16[3,128,2048]{2,1,0:T(8,128)(2,1)} %wk_hbm.1, bf16[3,128,2048]{2,1,0:T(8,128)(2,1)} %wv_hbm.1, bf16[512,512]{1,0:T(8,128)(2,1)} %wo_hbm.1), custom_call_target="tpu_custom_call" | custom-call | tf_op jit(solution)/shard_map/pallas_call | solution.py:905
  28.4 0.8 %shard_map.78 = (bf16[384,512]{1,0:T(8,128)(2,1)}, f32[2,384]{1,0:T(2,128)}) custom-call(bf16[384,512]{1,0:T(8,128)(2,1)S(1)} %get-tuple-element.4.proj_ref, f32[2,384]{1,0:T(2,128)S(1)} %get-tuple-element.5.logw_ref), custom_call_target="tpu_custom_call" | custom-call | tf_op jit(solution)/shard_map/pallas_call | solution.py:955
Async XLA Ops:
  0.6 0.7 %copy-start = (f32[2048]{0:T(1024)S(1)}, f32[2048]{0:T(1024)}, u32[]{:S(2)}) copy-start(f32[2048]{0:T(1024)} %param.7) | copy-start | bytes 24580

commit v2 on v1

--- a/solution.py
+++ b/solution.py
@@ -14,7 +14,7 @@
 NEG_BIG = -1e30
 CHUNKS = 2
 STORE_LIMIT = 8 * 1024 * 1024
-VMEM_LIMIT = 56098816
+VMEM_LIMIT = 60 * 1024 * 1024
 MESH = pl.DeviceIdType.MESH
 
 
@@ -495,8 +495,8 @@
     proj_ref, logw_ref,
     tok, gain, w_all, w_out, normed, acc, q1, q2, ctx1, ctx2, going, stream, qfar,
     answer, answer_far, lse_near, lse_far, back, back_far, back_lse, back_far_lse,
-    b0, b0_first, b1, b2, b3, out0, log0, part_o, part_l, mix, nat, lw_nat,
-    in_sem, gs, gr, fs, fr, ns, nr, as_, ar, ls, lr, bs, br, cs, cr, ms, mr,
+    b0, b0_first, b1, b2, b3, out0, log0, part_o, part_l, mix, nat, flat, lw_nat,
+    in_sem, one, ns, nr, br, cr, xr, dr, er,
 ):
     rows, width = tok.shape
     cols = wq_hbm.shape[1]
@@ -512,25 +512,25 @@
     upper = me >= classes
     lower = me < classes
 
+    gs, gr, fs, fr, as_, ar, ls, lr, bs, cs, xs, ds, es = [one.at[n] for n in range(13)]
     loads = {}
 
-    def load(name, src, dst):
-        loads[name] = pltpu.make_async_copy(src, dst, in_sem.at[len(loads)])
+    def load(name, src, dst, sem):
+        loads[name] = pltpu.make_async_copy(src, dst, in_sem.at[sem])
         loads[name].start()
 
     for c in range(classes):
         at = pl.ds(c * per, per)
-        load(("tok", c), tok_hbm.at[at], tok.at[at])
+        load(("tok", c), tok_hbm.at[at], tok.at[at], c)
         if c == 0:
-            load("gain", gain_hbm, gain)
-    slot = 0
+            load("gain", gain_hbm, gain, classes)
     weights = (
         (2, "q"), (2, "k"), (2, "v"), (1, "k"), (1, "v"), (0, "k"), (0, "v"), (1, "q"), (0, "q"))
-    for g, kind in weights:
+    for slot, (g, kind) in enumerate(weights):
         src = {"q": wq_hbm, "k": wk_hbm, "v": wv_hbm}[kind]
-        load((kind, g), src.at[g], w_all.at[slot * cols:(slot + 1) * cols])
-        slot += 1
-    load("out", wo_hbm, w_out)
+        sem = classes + (1 if slot < 3 else 2 if slot < 7 else 3)
+        load((kind, g), src.at[g], w_all.at[slot * cols:(slot + 1) * cols], sem)
+    load("out", wo_hbm, w_out, classes + 4)
 
     barrier = pltpu.get_barrier_semaphore()
     for k in range(1, n_sp):
@@ -597,18 +597,17 @@
             scale = lax.rsqrt(jnp.mean(x * x, axis=-1, keepdims=True) + 1e-06)
             normed[at, :] = (x * scale * gain[...]).astype(jnp.bfloat16)
 
-    def product(first, count):
-        for g, kind in weights[first:first + count]:
-            loads[kind, g].wait()
+    def product(first, count, sem):
+        part = w_all.at[first * cols:(first + count) * cols]
+        pltpu.make_async_copy(part, part, in_sem.at[classes + sem]).wait()
         return lax.dot_general(
-            normed[...], w_all[first * cols:(first + count) * cols, :], NT,
-            preferred_element_type=jnp.float32)
+            normed[...], part[...], NT, preferred_element_type=jnp.float32)
 
     def by_class(n, p):
         return acc[n, pl.ds(p, per, stride=classes), :].astype(jnp.bfloat16)
 
     scaling = jnp.bfloat16(1.0 / math.sqrt(HEAD_DIM))
-    got = product(0, 3)
+    got = product(0, 3, 1)
     for n in range(3):
         acc[n] = got[:, n * cols:(n + 1) * cols]
     for p in range(classes):
@@ -624,24 +623,24 @@
             src, dst, send, recv, device_id={"sp": sp}, device_id_type=MESH)
 
     def go(c, source):
-        return remote(going.at[c], stream.at[slice_of(source), :], gs.at[c], gr.at[source], base + c)
+        return remote(going.at[c], stream.at[slice_of(source), :], gs, gr, base + c)
 
     def go_far(c, source):
-        return remote(going.at[c, :, 0:cols], qfar.at[source], fs.at[c], fr.at[source], c)
+        return remote(going.at[c, :, 0:cols], qfar.at[source], fs, fr, c)
 
     def reply(e, source):
-        return remote(answer.at[e], back.at[source], as_.at[e], ar.at[source], base + e)
+        return remote(answer.at[e], back.at[source], as_, ar, base + e)
 
     def reply_lse(e, source):
-        return remote(lse_near.at[e], back_lse.at[source], ls.at[e], lr.at[source], base + e)
+        return remote(lse_near.at[e], back_lse.at[source], ls, lr, base + e)
 
     def reply_far(e, source):
         return remote(
-            answer_far.at[e], back_far.at[source], bs.at[e], br.at[source], classes + e)
+            answer_far.at[e], back_far.at[source], bs, br.at[source], classes + e)
 
     def reply_far_lse(e, source):
         return remote(
-            lse_far.at[e], back_far_lse.at[source], cs.at[e], cr.at[source], classes + e)
+            lse_far.at[e], back_far_lse.at[source], cs, cr.at[source], classes + e)
 
     def when(cond, f):
         @pl.when(cond)
@@ -654,6 +653,9 @@
 
     tail = tile - per
     full2 = pl.ds(0, classes)
+
+    even = lax.rem(me, 2) == 0
+    odd = lax.rem(me, 2) == 1
 
     def near(n):
         if n == 0:
@@ -662,19 +664,19 @@
             src, dst, by = ctx2.at[full2, tile:tile + per, :], ctx2.at[full2, tail:tile, :], 1
         else:
             src, dst, by = ctx2.at[full2, tile + per - tail:tile + per, :], ctx2.at[full2, 0:tail, :], 2
-        return by, remote(src, dst, ns.at[n], nr.at[n], me + by)
-
-    def near_start(n):
-        by, copy = near(n)
-        when(me + by < n_sp, copy.start)
+        return remote(src, dst, ns.at[n], nr.at[n], me + by)
+
+    sends = (me + 1 < n_sp, me + 1 < n_sp, me + 2 < n_sp)
+    gets = (me >= 1, me >= 1, me >= 2)
+
+    def near_start(n, side):
+        when(sends[n] & side, near(n).start)
 
     def near_sent(n):
-        by, copy = near(n)
-        when(me + by < n_sp, copy.wait_send)
+        when(sends[n], near(n).wait_send)
 
     def near_arrival(n):
-        by, copy = near(n)
-        when(me >= by, copy.wait_recv)
+        when(gets[n], near(n).wait_recv)
 
     pl.semaphore_wait(barrier, n_sp - 1 + n_tp - 1)
 
@@ -686,7 +688,7 @@
     each_peer(lambda e: go(e, mine).start())
     stream[slice_of(mine), :] = going[mine]
 
-    got = product(3, 4)
+    got = product(3, 4, 2)
     for n in range(2):
         acc[n] = got[:, n * cols:(n + 1) * cols]
     for p in range(classes):
@@ -694,11 +696,14 @@
             ctx2[p, tile:tile + per, n * cols:(n + 1) * cols] = by_class(n, p)
     ctx1[tile:tile + rows, :] = got[:, 2 * cols:4 * cols].astype(jnp.bfloat16)
 
-    got = product(7, 2)
+    got = product(7, 2, 3)
     acc[2] = got[:, 0:cols]
     for p in range(classes):
         q2[p] = by_class(2, p) * scaling
     q1[...] = got[:, cols:2 * cols].astype(jnp.bfloat16) * scaling
+    near_start(1, even)
+    near_start(2, even)
+    near_start(0, even)
 
     lane = lax.broadcasted_iota(jnp.int32, (1, cols), 1)
     lane_head = lane // HEAD_DIM
@@ -745,14 +750,16 @@
 
     for j in range(1, rows // tile):
         near_tile(j, b0)
-    near_start(1)
-    near_start(2)
-    near_start(0)
-
-    def go_arrival(k):
-        go(k, k).wait_recv()
-
-    each_peer(go_arrival)
+    near_start(2, odd)
+    near_start(1, odd)
+    near_start(0, odd)
+
+    others = classes - 1
+
+    def wait_bytes(ref, sem):
+        pltpu.make_async_copy(ref, ref, sem).wait()
+
+    wait_bytes(stream.at[0:others * per, :], gr)
     for k in range(classes):
         stop = near_keys(k)
         out, lse = attend(
@@ -766,8 +773,7 @@
 
     @pl.when(lower)
     def _():
-        for k in range(classes):
-            go_far(k, k).wait_recv()
+        wait_bytes(qfar, fr)
         for k in range(classes):
             first = far_keys(k)
             out, lse = attend(
@@ -776,13 +782,13 @@
             answer_far[k] = out.astype(jnp.bfloat16)
             pack(lse_far, k, lse)
         for k in range(classes):
-            reply_far(k, mine).start()
-            reply_far_lse(k, mine).start()
-
-    near_arrival(0)
+            turn = lax.rem(mine + k, classes)
+            reply_far(turn, mine).start()
+            reply_far_lse(turn, mine).start()
+
+    for n in range(3):
+        near_arrival(n)
     near_tile(0, b0_first)
-    near_arrival(1)
-    near_arrival(2)
     near_parts = []
     for p in range(classes):
         near_parts.append(attend(
@@ -797,7 +803,8 @@
         log = top + jnp.log(sum(jnp.exp(l - top) for l in logs))
         return log, sum(jnp.exp(l - log) * o for l, o in zip(logs, outs))
 
-    each_peer(lambda e: (reply(e, e).wait_recv(), reply_lse(e, e).wait_recv()))
+    wait_bytes(back.at[0:others], ar)
+    wait_bytes(back_lse.at[0:others], lr)
     for p in range(classes):
         at = pl.ds(p, per, stride=classes)
         log, out = merge(
@@ -805,17 +812,18 @@
             [out0[at, :], part_o[p], back[p].astype(jnp.float32)])
         part_l[p] = log
         part_o[p] = out
-
-    def spread(k, c):
+    turns = [lax.rem(mine + classes - k, classes) for k in range(classes)]
+
+    mate = tp + 1 - 2 * lax.rem(tp, 2)
+    across = lax.rem(tp + n_tp // 2, n_tp)
+
+    def hand(source, c, to, send, recv):
         return pltpu.make_async_remote_copy(
-            mix.at[tp, c], mix.at[tp, c], ms.at[k - 1, c], mr.at[k - 1, c],
-            device_id={"tp": lax.rem(tp + k, n_tp)}, device_id_type=MESH)
-
-    def spread_arrival(k, c):
-        source = lax.rem(tp + n_tp - k, n_tp)
-        return pltpu.make_async_remote_copy(
-            mix.at[source, c], mix.at[source, c], ms.at[k - 1, c], mr.at[k - 1, c],
-            device_id={"tp": lax.rem(tp + k, n_tp)}, device_id_type=MESH)
+            mix.at[source, c], mix.at[source, c], send, recv.at[c],
+            device_id={"tp": to}, device_id_type=MESH)
+
+    first_core = lax.rem(tp, 2) == 0
+    across_mate = lax.rem(mate + n_tp // 2, n_tp)
 
     def finish(c):
         @pl.when(upper)
@@ -829,48 +837,76 @@
             part_o[c] = out
 
         mix[tp, c] = part_o[c].astype(jnp.bfloat16)
-        lw_nat[pl.ds(c, per, stride=classes), :] = part_l[c]
-        for k in range(1, n_tp):
-            spread(k, c).start()
+
+        @pl.when(first_core)
+        def _():
+            hand(tp, c, across_mate, es, er).start()
+
+        hand(tp, c, across, xs, xr).start()
+        hand(tp, c, mate, ds, dr).start()
+
+    def forward(c):
+        @pl.when(~first_core)
+        def _():
+            hand(across, c, across, xs, xr).wait_recv()
+            hand(across, c, mate, ds, dr).start()
 
     def project_class(c):
-        for k in range(1, n_tp):
-            spread_arrival(k, c).wait_recv()
+        @pl.when(first_core)
+        def _():
+            hand(across, c, across, xs, xr).wait_recv()
+            wait_bytes(mix.at[0:2, 0], dr.at[c])
+
+        @pl.when(~first_core)
+        def _():
+            hand(across, c, across, es, er).wait_recv()
+            wait_bytes(mix.at[0, 0], dr.at[c])
         mixed = jnp.concatenate([mix[t, c] for t in range(n_tp)], axis=1)
         got = jnp.dot(mixed, w_out[...], preferred_element_type=jnp.float32)
         for n in range(nat.shape[0]):
-            nat[n, pl.ds(c, per, stride=classes), :] = got[:, n * LANES:(n + 1) * LANES]
-
-    finish(0)
-    finish(1)
+            nat[n, c] = got[:, n * LANES:(n + 1) * LANES]
+
+    for c in turns:
+        finish(c)
     loads["out"].wait()
-    for c in range(classes):
-        if c + 2 < classes:
-            finish(c + 2)
+    for p in range(classes):
+        lw_nat[pl.ds(p, per, stride=classes), :] = part_l[p]
+    for c in turns:
+        forward(c)
+    for c in turns:
         project_class(c)
     for n in range(nat.shape[0]):
-        proj_ref[:, n * LANES:(n + 1) * LANES] = nat[n].astype(jnp.bfloat16)
+        for p in range(classes):
+            flat[n, pl.ds(p, per, stride=classes), :] = nat[n, p]
+        proj_ref[:, n * LANES:(n + 1) * LANES] = flat[n].astype(jnp.bfloat16)
     for j in range(rows // tile):
         flipped = lw_nat[j * tile:(j + 1) * tile, :].T
         for h in range(heads):
             logw_ref[h:h + 1, j * tile:(j + 1) * tile] = flipped[h * HEAD_DIM:h * HEAD_DIM + 1, :]
 
-    for c in range(classes):
-        for k in range(1, n_tp):
-            spread(k, c).wait_send()
-    each_peer(lambda e: (
-        go(e, mine).wait_send(), reply(e, mine).wait_send(), reply_lse(e, mine).wait_send()))
+    wait_bytes(mix.at[0], xs)
+
+    @pl.when(first_core)
+    def _():
+        wait_bytes(mix.at[0], ds)
+        wait_bytes(mix.at[0], es)
+
+    @pl.when(~first_core)
+    def _():
+        wait_bytes(mix.at[0:2], ds)
+
+    wait_bytes(going.at[0:others], gs)
+    wait_bytes(answer.at[0:others], as_)
+    wait_bytes(lse_near.at[0:others], ls)
 
     @pl.when(upper)
     def _():
-        for c in range(classes):
-            go_far(c, mine).wait_send()
+        wait_bytes(going.at[:, :, 0:cols], fs)
 
     @pl.when(lower)
     def _():
-        for c in range(classes):
-            reply_far(c, mine).wait_send()
-            reply_far_lse(c, mine).wait_send()
+        wait_bytes(answer_far, bs)
+        wait_bytes(lse_far, cs)
 
     for n in range(3):
         near_sent(n)
@@ -904,7 +940,7 @@
     )
     results = pl.pallas_call(
         functools.partial(split_kernel, n_sp, n_tp, heads * n_tp),
-        out_shape=shapes,
+        out_shape=tuple(vmem(shape.shape, shape.dtype) for shape in shapes),
         in_specs=[pl.BlockSpec(memory_space=pltpu.HBM)] * 6,
         out_specs=(pl.BlockSpec(memory_space=pltpu.VMEM),) * 2,
         scratch_shapes=[
@@ -939,14 +975,11 @@
             vmem((classes, per, cols), f32),
             vmem((classes, per, cols), f32),
             vmem((n_tp, classes, per, cols), bf),
+            vmem((out_cols // LANES, classes, per, LANES), f32),
             vmem((out_cols // LANES, rows, LANES), f32),
             vmem((rows, cols), f32),
-            dma((11 + classes,)),
-            dma((classes,)), dma((classes,)), dma((classes,)), dma((classes,)),
-            dma((3,)), dma((3,)),
-            dma((classes,)), dma((classes,)), dma((classes,)), dma((classes,)),
-            dma((classes,)), dma((classes,)), dma((classes,)), dma((classes,)),
-            dma((n_tp - 1, classes)), dma((n_tp - 1, classes)),
+            dma((classes + 5,)), dma((13,)), dma((3,)), dma((3,)),
+            dma((classes,)), dma((classes,)), dma((classes,)), dma((classes,)), dma((classes,)),
         ],
         compiler_params=pltpu.CompilerParams(
             collective_id=0, has_side_effects=True, vmem_limit_bytes=VMEM_LIMIT
@@ -964,7 +997,7 @@
 
 def splits(n_sp, n_tp, rows, cols, out_cols):
     classes = n_sp // 2
-    if n_sp % 2 or classes != DILATIONS[1] or DILATIONS[2] % classes:
+    if n_tp != 4 or n_sp % 2 or classes != DILATIONS[1] or DILATIONS[2] % classes:
         return False
     if cols != LANES or LANES % HEAD_DIM or rows % (classes * 32) or rows % STEPS or out_cols % LANES:
         return False

time: 29.3 us -> 26.7 us (0.911)
  the two profiles are of different devices: /device:TPU:0 before, /device:TPU:16 now
where the time goes in v2:
time: 26.7 us; the launch traced here: 26.6 us
  Pallas kernels  25.9 us (97%)
  between operations  0.64 us (2%)
    pallas_call x1, Pallas kernels, split_call(): pl.pallas_call(functools.partial(split_kernel, n_sp, n_tp, heads * n_tp),...  25.2 us
    pallas_call x1, Pallas kernels, split_call(): pl.pallas_call(store, out_shape=shapes, in_specs=[pl.BlockSpec(memory_spa...  0.77 us

profile of v2, /device:TPU:16, one launch (start us, length us, event | category | flops | bytes accessed | tf_op | source)
XLA Modules:
  0.0 26.6 jit_solution(14940933232619049173)
XLA Ops:
  0.6 25.2 %shard_map.77 = (bf16[384,512]{1,0:T(8,128)(2,1)S(1)}, f32[2,384]{1,0:T(2,128)S(1)}) custom-call(bf16[384,2048]{1,0:T(8,128)(2,1)} %tok_hbm.1, f32[1,2048]{1,0:T(1,128)} %bitcast.1, bf16[3,128,2048]{2,1,0:T(8,128)(2,1)} %wq_hbm.1, bf16[3,128,2048]{2,1,0:T(8,128)(2,1)} %wk_hbm.1, bf16[3,128,2048]{2,1,0:T(8,128)(2,1)} %wv_hbm.1, bf16[512,512]{1,0:T(8,128)(2,1)} %wo_hbm.1), custom_call_target="tpu_custom_call" | custom-call | tf_op jit(solution)/shard_map/pallas_call | solution.py:941
  25.8 0.8 %shard_map.78 = (bf16[384,512]{1,0:T(8,128)(2,1)}, f32[2,384]{1,0:T(2,128)}) custom-call(bf16[384,512]{1,0:T(8,128)(2,1)S(1)} %get-tuple-element.4.proj_ref, f32[2,384]{1,0:T(2,128)S(1)} %get-tuple-element.5.logw_ref), custom_call_target="tpu_custom_call" | custom-call | tf_op jit(solution)/shard_map/pallas_call | solution.py:988
